TPU v7x, 32 devices: a whole 2x2x4 slice. The times are simulated.
32 devices in a mesh: ep: 8 (over z, y), tp: 4 (over x, core).
Axes of the slice: x: 2, y: 2, z: 4, core: 2. Of those that a mesh axis runs over, the one named last changes fastest.
Arguments:
- tokens: bfloat16 [2048, 1024], P('ep'), may hold values from -6 to 6
- cotangent: bfloat16 [2048, 1024], P('ep'), may hold values from -1.5 to 1.5
- routing: int32 [2048, 2], P('ep'), may hold values from 0 to 15, all different within a row; in each aligned block of 256 rows (0 to 255, 256 to 511, ...) at most 96 rows name the same one
- gate_weights: float32 [2048, 2], P('ep'), may hold values from 0.1 to 0.9
- gate_proj: bfloat16 [16, 1024, 512], P('ep', None, 'tp'), may hold values from -0.1875 to 0.1875
- up_proj: bfloat16 [16, 1024, 512], P('ep', None, 'tp'), may hold values from -0.1875 to 0.1875
- down_proj: bfloat16 [16, 512, 1024], P('ep', 'tp'), may hold values from -0.25 to 0.25
Outputs:
- tokens_grad: bfloat16 [2048, 1024], P('ep')
- gates_grad: float32 [2048, 2], P('ep')
- gate_proj_grad: float32 [16, 1024, 512], P('ep', None, 'tp')
- up_proj_grad: float32 [16, 1024, 512], P('ep', None, 'tp')
- down_proj_grad: float32 [16, 512, 1024], P('ep', 'tp')
Inputs may be any that keep to these rules, and one draw needn't show every extreme that they name: `routing`: each row names 2 different experts; every expert is named by some row; within each aligned block of 256 rows (the tokens of one index of ep) no expert is named by more than 96 rows, a bound that some block reaches.
All inputs are finite; a program needn't handle non-finite values.
Results may differ from a plain program's by a relative error of at most 0.0015.
Values may be sent and summed in bfloat16 or wider, within the bound.
A program may use at most 128 MiB of HBM per device.

v0:
```python
import jax
import jax.numpy as jnp
from jax import lax
from jax.sharding import PartitionSpec as P


def expert_terms(expert_rows, expert_scaled, gate_proj, up_proj, down_proj):
    gate_pre = jnp.einsum(
        "erd,edf->erf", expert_rows, gate_proj, preferred_element_type=jnp.float32
    ).astype(jnp.bfloat16)
    up_pre = jnp.einsum(
        "erd,edf->erf", expert_rows, up_proj, preferred_element_type=jnp.float32
    ).astype(jnp.bfloat16)
    gate_pre, up_pre = lax.optimization_barrier((gate_pre, up_pre))
    hidden_grad = jnp.einsum(
        "erd,efd->erf", expert_scaled, down_proj, preferred_element_type=jnp.float32
    )
    gate_wide = gate_pre.astype(jnp.float32)
    up_wide = up_pre.astype(jnp.float32)
    sigmoid_gate = jax.nn.sigmoid(gate_wide)
    activated = gate_wide * sigmoid_gate
    hidden = activated * up_wide
    product = jnp.sum(hidden_grad * hidden, axis=-1)
    gate_pre_grad = (
        hidden_grad * up_wide * sigmoid_gate * (1.0 + gate_wide * (1.0 - sigmoid_gate))
    ).astype(jnp.bfloat16)
    up_pre_grad = (hidden_grad * activated).astype(jnp.bfloat16)
    input_grad = jnp.einsum(
        "erf,edf->erd", gate_pre_grad, gate_proj, preferred_element_type=jnp.float32
    )
    input_grad = input_grad + jnp.einsum(
        "erf,edf->erd", up_pre_grad, up_proj, preferred_element_type=jnp.float32
    )
    down_grad = jnp.einsum(
        "erf,erd->efd",
        hidden.astype(jnp.bfloat16),
        expert_scaled,
        preferred_element_type=jnp.float32,
    )
    gate_grad = jnp.einsum(
        "erd,erf->edf", expert_rows, gate_pre_grad, preferred_element_type=jnp.float32
    )
    up_grad = jnp.einsum(
        "erd,erf->edf", expert_rows, up_pre_grad, preferred_element_type=jnp.float32
    )
    return (input_grad, product, gate_grad, up_grad, down_grad)


def slot_shards(tokens, cotangent, routing, gate_weights, gate_proj, up_proj, down_proj):
    token_count, model_width = tokens.shape
    top_count = routing.shape[1]
    local_experts = gate_proj.shape[0]
    groups = lax.axis_size("ep")
    members = lax.axis_size("tp")
    experts = local_experts * groups
    capacity = members * (
        (3 * token_count * top_count + experts * members - 1) // (experts * members)
    )
    slot_count = experts * capacity
    pair_count = token_count * top_count
    pair_expert = routing.reshape(pair_count)
    onehot = (pair_expert[:, None] == jnp.arange(experts, dtype=jnp.int32)[None, :]).astype(
        jnp.int32
    )
    position = jnp.sum(jnp.cumsum(onehot, axis=0) * onehot, axis=1) - 1
    pair_slot = pair_expert * capacity + position
    pair_number = jnp.arange(pair_count, dtype=jnp.int32)
    owner_pair = jnp.zeros((slot_count,), jnp.int32).at[pair_slot].set(pair_number)
    filled = jnp.zeros((slot_count,), jnp.int32).at[pair_slot].set(1) > 0
    owner_token = owner_pair // top_count
    slot_weight = jnp.where(filled, gate_weights.reshape(pair_count)[owner_pair], 0.0)
    send_rows = jnp.where(filled[:, None], tokens[owner_token], jnp.zeros((), jnp.bfloat16))
    send_scaled = (slot_weight[:, None] * cotangent[owner_token].astype(jnp.float32)).astype(
        jnp.bfloat16
    )
    layout = (groups, local_experts, capacity, model_width)
    send_rows = send_rows.reshape(layout)
    send_scaled = send_scaled.reshape(layout)
    quarter = capacity // members
    quarter_start = lax.axis_index("tp") * quarter
    part_rows = lax.dynamic_slice_in_dim(send_rows, quarter_start, quarter, 2)
    part_scaled = lax.dynamic_slice_in_dim(send_scaled, quarter_start, quarter, 2)
    landed = (
        lax.all_to_all(part_rows, "ep", split_axis=0, concat_axis=0, tiled=True),
        lax.all_to_all(part_scaled, "ep", split_axis=0, concat_axis=0, tiled=True),
    )
    recv_rows, recv_scaled = (
        lax.all_gather(landed[0], "tp", axis=2, tiled=True),
        lax.all_gather(landed[1], "tp", axis=2, tiled=True),
    )
    expert_rows = recv_rows.transpose(1, 0, 2, 3).reshape(
        local_experts, groups * capacity, model_width
    )
    expert_scaled = recv_scaled.transpose(1, 0, 2, 3).reshape(
        local_experts, groups * capacity, model_width
    )
    input_grad, product, gate_grad, up_grad, down_grad = expert_terms(
        expert_rows, expert_scaled, gate_proj, up_proj, down_proj
    )
    input_grad = input_grad.reshape(local_experts, groups, capacity, model_width).transpose(
        1, 0, 2, 3
    )
    product = product.reshape(local_experts, groups, capacity).transpose(1, 0, 2)
    back_grad, back_product = (
        lax.all_to_all(input_grad, "ep", split_axis=0, concat_axis=0, tiled=True),
        lax.all_to_all(product, "ep", split_axis=0, concat_axis=0, tiled=True),
    )
    local_slot = position
    present = (local_slot >= 0) & (local_slot < capacity)
    back_index = pair_expert * capacity + jnp.clip(local_slot, 0, capacity - 1)
    pair_grad = jnp.where(
        present[:, None], back_grad.reshape(experts * capacity, model_width)[back_index], 0.0
    )
    pair_product = jnp.where(present, back_product.reshape(experts * capacity)[back_index], 0.0)
    token_grad = jnp.sum(pair_grad.reshape(token_count, top_count, model_width), axis=1)
    total_grad, total_product = lax.psum((token_grad, pair_product), "tp")
    tokens_grad = total_grad.astype(jnp.bfloat16)
    gates_grad = (total_product / gate_weights.reshape(pair_count)).reshape(token_count, top_count)
    return (tokens_grad, gates_grad, gate_grad, up_grad, down_grad)


def dense_shards(tokens, cotangent, routing, gate_weights, gate_proj, up_proj, down_proj):
    token_count, model_width = tokens.shape
    local_experts = gate_proj.shape[0]
    groups = lax.axis_size("ep")
    members = lax.axis_size("tp")
    experts = local_experts * groups
    all_axes = ("ep", "tp")
    quarter = token_count // members
    quarter_start = lax.axis_index("tp") * quarter
    both = jnp.concatenate(
        [
            lax.dynamic_slice_in_dim(tokens, quarter_start, quarter, 0),
            lax.dynamic_slice_in_dim(cotangent, quarter_start, quarter, 0),
        ],
        axis=1,
    )
    all_both = lax.all_gather(both, all_axes, axis=0, tiled=True)
    chosen = routing[:, :, None] == jnp.arange(experts, dtype=jnp.int32)[None, None, :]
    weights = jnp.sum(jnp.where(chosen, gate_weights[:, :, None], 0.0), axis=1)
    all_weights = lax.all_gather(weights, "ep", axis=0, tiled=True)
    first_expert = lax.axis_index("ep") * local_experts
    my_weights = lax.dynamic_slice_in_dim(all_weights, first_expert, local_experts, 1)
    all_tokens = all_both[:, :model_width]
    all_cotangent = all_both[:, model_width:].astype(jnp.float32)
    rows = jnp.broadcast_to(all_tokens[None], (local_experts,) + all_tokens.shape)
    scaled = (my_weights.T[:, :, None] * all_cotangent[None]).astype(jnp.bfloat16)
    input_grad, product, gate_grad, up_grad, down_grad = expert_terms(
        rows, scaled, gate_proj, up_proj, down_proj
    )
    partial = jnp.sum(input_grad, axis=0)
    own = jnp.zeros((token_count * groups, experts), jnp.float32)
    own = lax.dynamic_update_slice_in_dim(own, product.T, first_expert, 1)
    part_grad = lax.psum_scatter(partial, all_axes, scatter_dimension=0, tiled=True)
    part_product = lax.psum_scatter(own, all_axes, scatter_dimension=0, tiled=True)
    tokens_grad = lax.all_gather(part_grad.astype(jnp.bfloat16), "tp", axis=0, tiled=True)
    block_product = lax.all_gather(part_product, "tp", axis=0, tiled=True)
    pair_product = jnp.sum(jnp.where(chosen, block_product[:, None, :], 0.0), axis=2)
    gates_grad = pair_product / gate_weights
    return (tokens_grad, gates_grad, gate_grad, up_grad, down_grad)


def shards(tokens, cotangent, routing, gate_weights, gate_proj, up_proj, down_proj):
    token_count = tokens.shape[0]
    experts = gate_proj.shape[0] * lax.axis_size("ep")
    members = lax.axis_size("tp")
    fair = token_count * routing.shape[1] // experts
    dense = token_count <= 8 * fair and token_count % members == 0
    plan = dense_shards if dense else slot_shards
    return plan(tokens, cotangent, routing, gate_weights, gate_proj, up_proj, down_proj)


def solution(mesh):
    in_specs = (
        P("ep", None),
        P("ep", None),
        P("ep", None),
        P("ep", None),
        P("ep", None, "tp"),
        P("ep", None, "tp"),
        P("ep", "tp", None),
    )
    out_specs = (
        P("ep", None),
        P("ep", None),
        P("ep", None, "tp"),
        P("ep", None, "tp"),
        P("ep", "tp", None),
    )
    return jax.shard_map(shards, mesh=mesh, in_specs=in_specs, out_specs=out_specs, check_vma=False)
```

profile of v0, /device:TPU:0, one launch (start us, length us, event | category | flops | bytes accessed | tf_op | source)
XLA Modules:
  0.0 418.2 jit_solution(15202121153911401712)
XLA Ops:
  7.2 0.0 copy-start
  7.2 0.0 all-gather.3.cloned.1.call-start
  7.2 1.0 constant_dynamic-slice_fusion
  8.3 0.7 pad_maximum_fusion
  9.0 0.0 all-gather.3.cloned.1.call-update
  9.0 0.0 reduce-scatter.7.cloned.1.call-start
  9.1 0.7 select_reduce_fusion.1
  9.8 32.6 %all_gather.12 = f32[2048,16]{0,1:T(8,128)S(1)} all-gather(f32[256,16]{0,1:T(8,128)S(1)} %select_reduce_fusion.1), channel_id=1, replica_groups=mesh['ep'=8,'tp'=4] {'ep'}, dimensions={0}, use_global_device_ids=true | all-gather | bytes 147456 | tf_op jit(solution)/shard_map/all_gather | solution.py:141
  42.4 48.9 %all-gather.3.cloned.1.call-done = bf16[2048,2048]{1,0:T(8,128)(2,1)} async-done(((bf16[64,2048]{1,0:T(8,128)(2,1)}), bf16[2048,2048]{1,0:T(8,128)(2,1)}) %all-gather.3.cloned.1.call-update) | async-done | bytes 8388624 | tf_op jit(solution)/shard_map/all_gather | solution.py:138
  91.3 7.5 %fusion.29 = (bf16[2048,1024]{1,0:T(8,128)(2,1)}, f32[2048,1024]{1,0:T(8,128)}) fusion(bf16[2048,2048]{1,0:T(8,128)(2,1)} %all-gather.3.cloned.1.call-done), kind=kLoop, calls=%fused_computation.42 | loop fusion | flops 2097152 | bytes 20971520 | tf_op jit(solution)/shard_map/slice | solution.py:144
  98.8 0.0 copy-start.4
  98.8 6.5 %copy.60 = bf16[2048,1024]{0,1:T(8,128)(2,1)} copy(bf16[2048,1024]{1,0:T(8,128)(2,1)} %get-tuple-element.9) | data formatting | bytes 8388608 | tf_op jit(solution)/shard_map/slice | solution.py:144
  105.4 0.0 copy-done.4
  105.4 0.0 slice-start
  105.4 3.7 fusion.17
  109.0 0.0 copy-done
  109.1 0.0 copy-start.8
  109.1 0.0 slice-start.1
  109.1 0.0 copy-start.7
  109.1 3.9 fusion.14
  113.0 0.0 copy-start.2
  113.0 0.0 copy-done.8
  113.0 0.0 slice-done
  113.0 0.0 slice-done.1
  113.1 0.0 copy-done.7
  113.1 5.0 %multiply_reduce_fusion = (f32[2,2048]{1,0:T(2,128)S(1)}, bf16[2,2048,128]{1,2,0:T(8,128)(2,1)}, f32[2,2048,128]{1,2,0:T(8,128)S(1)}) fusion(bf16[2,2048,128]{1,2,0:T(8,128)(2,1)S(1)} %fusion.17, bf16[2,2048,128]{1,2,0:T(8,128)(2,1)S(1)} %fusion.14, bf16[2,128,1024]{2,1,0:T(8,128)(2,1)S(1)} %copy-done.7, f32[2048,1024]{1,0:T(8,128)S(1)} %bitcast.16, ...), kind=kOutput, calls=%fused_computation.31 | convolution fusion | flops 1090514944 | bytes 14188544 | tf_op jit(solution)/shard_map/erd,efd->erf/dot_general | solution.py:15
  118.1 0.0 copy-done.2
  118.1 1.3 copy.78
  119.5 0.0 reduce-scatter.7.cloned.1.call-update
  119.5 0.2 reduce-scatter.5.cloned.1.call-start
  119.7 9.3 %fusion.30 = f32[2,2048,1024]{2,1,0:T(8,128)} fusion(bf16[2,2048,128]{1,2,0:T(8,128)(2,1)} %get-tuple-element.12, bf16[2,1024,128]{2,1,0:T(8,128)(2,1)S(1)} %copy-done), kind=kOutput, calls=%fused_computation.43 | convolution fusion | flops 1073741824 | bytes 18350080 | tf_op jit(solution)/shard_map/erf,edf->erd/dot_general | solution.py:28
  129.1 11.5 %add_reduce_fusion = f32[2048,1024]{1,0:T(8,128)} fusion(f32[2,2048,1024]{2,1,0:T(8,128)} %fusion.30, bf16[2,1024,128]{2,1,0:T(8,128)(2,1)S(1)} %copy-done.4, f32[2,2048,128]{1,2,0:T(8,128)S(1)} %get-tuple-element.13, bf16[2,2048,128]{1,2,0:T(8,128)(2,1)} %copy-done.2), kind=kOutput, calls=%fused_computation | convolution fusion | flops 1083703296 | bytes 28835840 | tf_op jit(solution)/shard_map/erf,edf->erd/dot_general | solution.py:31
  140.6 0.0 reduce-scatter.5.cloned.1.call-update
  140.6 0.0 copy-start.1
  140.6 0.0 copy-start.3
  140.6 0.0 slice-start.2
  140.6 6.0 %fusion.8 = f32[2,1024,128]{2,1,0:T(8,128)} fusion(bf16[2,2048,128]{1,2,0:T(8,128)(2,1)} %get-tuple-element.12, bf16[2048,1024]{0,1:T(8,128)(2,1)} %copy.60), kind=kOutput, calls=%fused_computation.11 | convolution fusion | flops 1073741824 | bytes 6291456 | tf_op jit(solution)/shard_map/erd,erf->edf/dot_general | solution.py:40
  146.6 0.0 copy-done.1
  146.6 0.0 copy-done.3
  146.6 0.0 slice-start.3
  146.6 0.0 copy-start.9
  146.6 3.4 fusion.6
  150.0 0.0 slice-done.2
  150.0 0.0 slice-done.3
  150.0 0.0 copy-done.9
  150.0 0.0 copy-start.5
  150.0 0.0 copy-start.6
  150.0 3.2 fusion
  153.2 101.5 %reduce-scatter.7.cloned.1.call-done = f32[64,16]{1,0:T(8,128)} async-done(((f32[2048,16]{1,0:T(8,128)}), f32[64,16]{1,0:T(8,128)}) %reduce-scatter.7.cloned.1.call-update) | async-done | bytes 4112
  254.8 0.8 copy.79
  255.6 5.2 %all-gather = f32[4,64,16]{1,2,0:T(8,128)S(1)} all-gather(f32[1,64,16]{1,2,0:T(8,128)S(1)} %bitcast.19), channel_id=1, replica_groups=mesh['ep'=8,'tp'=4] {'tp'}, dimensions={0}, use_global_device_ids=true | all-gather | bytes 20480 | tf_op jit(solution)/shard_map/all_gather | solution.py:157
  260.8 0.1 reshape.17
  260.9 0.0 copy-done.5
  260.9 0.0 copy-done.6
  260.9 0.6 div.7
  261.5 141.9 %reduce-scatter.5.cloned.1.call-done = f32[64,1024]{1,0:T(8,128)} async-done(((f32[2048,1024]{1,0:T(8,128)}), f32[64,1024]{1,0:T(8,128)}) %reduce-scatter.5.cloned.1.call-update) | async-done | bytes 262160 | tf_op jit(solution)/shard_map/reduce_scatter | solution.py:154
  403.4 1.0 convert_element_type.38
  404.4 6.5 %all_gather.14 = bf16[256,1024]{1,0:T(8,128)(2,1)S(1)} all-gather(bf16[64,1024]{1,0:T(8,128)(2,1)S(1)} %convert_element_type.38), channel_id=1, replica_groups=mesh['ep'=8,'tp'=4] {'tp'}, dimensions={0}, use_global_device_ids=true | all-gather | bytes 655360 | tf_op jit(solution)/shard_map/all_gather | solution.py:156
  410.9 0.8 copy.82
  (7 shorter events, 0.1 us)
Async XLA Ops:
  7.2 101.9 %copy-start = (bf16[2,1024,128]{2,1,0:T(8,128)(2,1)S(1)}, bf16[2,1024,128]{2,1,0:T(8,128)(2,1)}, u32[]{:S(2)}) copy-start(bf16[2,1024,128]{2,1,0:T(8,128)(2,1)} %param.11) | copy-start | bytes 1572868
  7.2 84.2 %all-gather.3.cloned.1.call-start = ((), (), s32[]{:S(2)}) async-start(), calls=%async_computation.2 | async-start | bytes 8650752 | tf_op jit(solution)/shard_map/all_gather | solution.py:138
  9.0 245.7 %reduce-scatter.7.cloned.1.call-start = ((), (), s32[]{:S(2)}) async-start(), calls=%async_computation.4 | async-start | bytes 1081344
  98.8 6.6 %copy-start.4 = (bf16[2,1024,128]{2,1,0:T(8,128)(2,1)S(1)}, bf16[2,1024,128]{2,1,0:T(8,128)(2,1)}, u32[]{:S(2)}) copy-start(bf16[2,1024,128]{2,1,0:T(8,128)(2,1)} %param.12) | copy-start | bytes 1572868
  105.4 7.7 %slice-start = ((s8[8388608]{0:T(1024)(128)(4,1)}), s8[4194304]{0:T(1024)(128)(4,1)S(1)}, s32[]{:S(2)}) async-start(s8[8388608]{0:T(1024)(128)(4,1)} %bitcast.15), calls=%async_computation.5 | async-start | bytes 8388608
  109.1 4.0 copy-start.8
  109.1 4.0 slice-start.1
  109.1 4.0 copy-start.7
  113.0 5.1 %copy-start.2 = (bf16[2,2048,128]{1,2,0:T(8,128)(2,1)}, bf16[2,2048,128]{1,2,0:T(8,128)(2,1)S(1)}, u32[]{:S(2)}) copy-start(bf16[2,2048,128]{1,2,0:T(8,128)(2,1)S(1)} %fusion.14) | copy-start | bytes 3145732
  119.5 283.9 %reduce-scatter.5.cloned.1.call-start = ((), (), s32[]{:S(2)}) async-start(), calls=%async_computation.3 | async-start | bytes 8650752 | tf_op jit(solution)/shard_map/reduce_scatter | solution.py:154
  140.6 6.0 %copy-start.1 = (bf16[2048,1024]{0,1:T(8,128)(2,1)S(1)}, bf16[2048,1024]{0,1:T(8,128)(2,1)}, u32[]{:S(2)}) copy-start(bf16[2048,1024]{0,1:T(8,128)(2,1)} %copy.60) | copy-start | bytes 12582916
  140.6 6.0 %copy-start.3 = (bf16[2,2048,128]{1,2,0:T(8,128)(2,1)S(1)}, bf16[2,2048,128]{1,2,0:T(8,128)(2,1)}, u32[]{:S(2)}) copy-start(bf16[2,2048,128]{1,2,0:T(8,128)(2,1)} %copy-done.2) | copy-start | bytes 3145732
  140.6 9.4 %slice-start.2 = ((s8[8388608]{0:T(1024)(128)(4,1)}), s8[4194304]{0:T(1024)(128)(4,1)S(1)}, s32[]{:S(2)}) async-start(s8[8388608]{0:T(1024)(128)(4,1)} %bitcast.17), calls=%async_computation.7 | async-start | bytes 8388608
  146.6 3.4 slice-start.3
  146.6 3.4 copy-start.9
  150.0 110.9 %copy-start.5 = (s32[256,2]{0,1:T(2,128)S(1)}, s32[256,2]{0,1:T(2,128)}, u32[]{:S(2)}) copy-start(s32[256,2]{0,1:T(2,128)} %param.9) | copy-start | bytes 6148
  150.0 110.9 %copy-start.6 = (f32[256,2]{0,1:T(2,128)S(1)}, f32[256,2]{0,1:T(2,128)}, u32[]{:S(2)}) copy-start(f32[256,2]{0,1:T(2,128)} %param.10) | copy-start | bytes 6148
Sparse Core Ops, SparseCore 0:
  11.4 79.8 all-gather.2
  119.6 135.1 reduce-scatter.6
  257.1 146.3 reduce-scatter.4
where the time goes:
time: 419 us; the launch traced here: 418 us
  waiting for transfers between devices  292 us (70%)
  matrix products  46 us (11%)
  blocking collectives  44.3 us (11%)
  between operations  14 us (3%)
  local copies, waits for them, and re-layouts  10.7 us (3%)
  other arithmetic  10.5 us (3%)
    reduce_scatter x1, waiting for transfers between devices, dense_shards(): lax.psum_scatter(partial, all_axes, scatter_dimension=0, tiled=True)  142 us
    unnamed x4, waiting for transfers between devices  102 us
    all_gather x1, waiting for transfers between devices, dense_shards(): all_both = lax.all_gather(both, all_axes, axis=0, tiled=True)  48.9 us
    all_gather x1, blocking collectives, dense_shards(): all_weights = lax.all_gather(weights, 'ep', axis=0, tiled=True)  32.6 us
    dot_general x1, matrix products, expert_terms(): jnp.einsum('erf,edf->erd', up_pre_grad, up_proj, preferred_element_type=j...  11.5 us
    dot_general x1, matrix products, expert_terms(): jnp.einsum('erf,edf->erd', gate_pre_grad, gate_proj, preferred_element_ty...  9.35 us
  transfers between devices with their start and end apart: 3, of which 3 were waited for; matrix products, arithmetic and copies ran while one was open for 9% of the time, Pallas kernels for 0%

commit v1 on v0

--- a/solution.py
+++ b/solution.py
@@ -138,7 +138,12 @@
     all_both = lax.all_gather(both, all_axes, axis=0, tiled=True)
     chosen = routing[:, :, None] == jnp.arange(experts, dtype=jnp.int32)[None, None, :]
     weights = jnp.sum(jnp.where(chosen, gate_weights[:, :, None], 0.0), axis=1)
-    all_weights = lax.all_gather(weights, "ep", axis=0, tiled=True)
+    ring = [weights]
+    for hop in range(7):
+        ring.append(lax.ppermute(ring[-1], "ep", [(dev, (dev + 1) % 8) for dev in range(8)]))
+    all_weights = jnp.roll(
+        jnp.concatenate(ring[::-1], axis=0), (lax.axis_index("ep") + 1) * ring[0].shape[0], axis=0
+    )
     first_expert = lax.axis_index("ep") * local_experts
     my_weights = lax.dynamic_slice_in_dim(all_weights, first_expert, local_experts, 1)
     all_tokens = all_both[:, :model_width]

time: 419 us -> 419 us (level)
  blocking collectives: 44.3 us -> 11.7 us
  waiting for transfers between devices: 292 us -> 322 us
    ppermute x0 -> x7, waiting for transfers between devices: none -> 44.3 us  [dense_shards(): lax.ppermute(ring[-1], 'ep', [(dev, (dev + 1) % 8) for dev in range(8)])]
    all_gather x1 -> x0, blocking collectives: 32.6 us -> none  [dense_shards(): all_weights = lax.all_gather(weights, 'ep', axis=0, tiled=True)]
    all_gather x1, waiting for transfers between devices: 48.9 us -> 34.1 us  [dense_shards(): all_both = lax.all_gather(both, all_axes, axis=0, tiled=True)]
  transfers between devices with their start and end apart: 3 -> 10, of which waited for: 3 -> 10; matrix products, arithmetic and copies ran while one was open for 9% -> 9% of each run, Pallas kernels for 0% -> 0%
where the time goes in v1:
time: 419 us; the launch traced here: 418 us
  waiting for transfers between devices  322 us (77%)
  matrix products  46 us (11%)
  between operations  14.1 us (3%)
  blocking collectives  11.7 us (3%)
  local copies, waits for them, and re-layouts  11 us (3%)
  other arithmetic  10.5 us (3%)
    reduce_scatter x1, waiting for transfers between devices, dense_shards(): lax.psum_scatter(partial, all_axes, scatter_dimension=0, tiled=True)  142 us
    unnamed x4, waiting for transfers between devices  102 us
    ppermute x7, waiting for transfers between devices, dense_shards(): lax.ppermute(ring[-1], 'ep', [(dev, (dev + 1) % 8) for dev in range(8)])  44.3 us
    all_gather x1, waiting for transfers between devices, dense_shards(): all_both = lax.all_gather(both, all_axes, axis=0, tiled=True)  34.1 us
    dot_general x1, matrix products, expert_terms(): jnp.einsum('erf,edf->erd', up_pre_grad, up_proj, preferred_element_type=j...  11.5 us
    dot_general x1, matrix products, expert_terms(): jnp.einsum('erf,edf->erd', gate_pre_grad, gate_proj, preferred_element_ty...  9.35 us
  transfers between devices with their start and end apart: 10, of which 10 were waited for; matrix products, arithmetic and copies ran while one was open for 9% of the time, Pallas kernels for 0%

profile of v1, /device:TPU:0, one launch (start us, length us, event | category | flops | bytes accessed | tf_op | source)
XLA Modules:
  0.0 418.1 jit_solution(1673205589641829222)
XLA Ops:
  7.2 0.0 copy-start
  7.2 0.0 all-gather.3.cloned.1.call-start
  7.2 1.0 constant_dynamic-slice_fusion
  8.3 0.7 pad_maximum_fusion
  9.0 0.0 all-gather.3.cloned.1.call-update
  9.0 0.0 reduce-scatter.7.cloned.1.call-start
  9.1 0.7 select_reduce_fusion.1
  9.8 3.0 collective-permute-start
  12.8 4.8 %collective-permute-done = f32[256,16]{0,1:T(8,128)S(1)} collective-permute-done((f32[256,16]{0,1:T(8,128)S(1)}, f32[256,16]{0,1:T(8,128)S(1)}, u32[]{:S(2)}, u32[]{:S(2)}) %collective-permute-start) | collective-permute-done | bytes 16416 | tf_op jit(solution)/shard_map/ppermute | solution.py:143
  17.6 0.0 collective-permute-start.1
  17.6 6.4 %collective-permute-done.1 = f32[256,16]{0,1:T(8,128)S(1)} collective-permute-done((f32[256,16]{0,1:T(8,128)S(1)}, f32[256,16]{0,1:T(8,128)S(1)}, u32[]{:S(2)}, u32[]{:S(2)}) %collective-permute-start.1) | collective-permute-done | bytes 16416 | tf_op jit(solution)/shard_map/ppermute | solution.py:143
  24.0 0.0 collective-permute-start.2
  24.0 6.5 %collective-permute-done.2 = f32[256,16]{0,1:T(8,128)S(1)} collective-permute-done((f32[256,16]{0,1:T(8,128)S(1)}, f32[256,16]{0,1:T(8,128)S(1)}, u32[]{:S(2)}, u32[]{:S(2)}) %collective-permute-start.2) | collective-permute-done | bytes 16416 | tf_op jit(solution)/shard_map/ppermute | solution.py:143
  30.5 0.0 collective-permute-start.3
  30.5 6.5 %collective-permute-done.3 = f32[256,16]{0,1:T(8,128)S(1)} collective-permute-done((f32[256,16]{0,1:T(8,128)S(1)}, f32[256,16]{0,1:T(8,128)S(1)}, u32[]{:S(2)}, u32[]{:S(2)}) %collective-permute-start.3) | collective-permute-done | bytes 16416 | tf_op jit(solution)/shard_map/ppermute | solution.py:143
  37.0 0.0 collective-permute-start.4
  37.0 6.6 %collective-permute-done.4 = f32[256,16]{0,1:T(8,128)S(1)} collective-permute-done((f32[256,16]{0,1:T(8,128)S(1)}, f32[256,16]{0,1:T(8,128)S(1)}, u32[]{:S(2)}, u32[]{:S(2)}) %collective-permute-start.4) | collective-permute-done | bytes 16416 | tf_op jit(solution)/shard_map/ppermute | solution.py:143
  43.6 0.0 collective-permute-start.5
  43.7 6.9 %collective-permute-done.5 = f32[256,16]{0,1:T(8,128)S(1)} collective-permute-done((f32[256,16]{0,1:T(8,128)S(1)}, f32[256,16]{0,1:T(8,128)S(1)}, u32[]{:S(2)}, u32[]{:S(2)}) %collective-permute-start.5) | collective-permute-done | bytes 16416 | tf_op jit(solution)/shard_map/ppermute | solution.py:143
  50.6 0.0 collective-permute-start.6
  50.6 6.6 %collective-permute-done.6 = f32[256,16]{0,1:T(8,128)S(1)} collective-permute-done((f32[256,16]{0,1:T(8,128)S(1)}, f32[256,16]{0,1:T(8,128)S(1)}, u32[]{:S(2)}, u32[]{:S(2)}) %collective-permute-start.6) | collective-permute-done | bytes 16416 | tf_op jit(solution)/shard_map/ppermute | solution.py:143
  57.3 0.1 dynamic-slice_bitcast_fusion
  57.4 34.1 %all-gather.3.cloned.1.call-done = bf16[2048,2048]{1,0:T(8,128)(2,1)} async-done(((bf16[64,2048]{1,0:T(8,128)(2,1)}), bf16[2048,2048]{1,0:T(8,128)(2,1)}) %all-gather.3.cloned.1.call-update) | async-done | bytes 8388624 | tf_op jit(solution)/shard_map/all_gather | solution.py:138
  91.5 7.5 %fusion.29 = (bf16[2048,1024]{1,0:T(8,128)(2,1)}, f32[2048,1024]{1,0:T(8,128)}) fusion(bf16[2048,2048]{1,0:T(8,128)(2,1)} %all-gather.3.cloned.1.call-done), kind=kLoop, calls=%fused_computation.58 | loop fusion | flops 2097152 | bytes 20971520 | tf_op jit(solution)/shard_map/slice | solution.py:149
  99.0 6.6 %copy.60 = bf16[2048,1024]{0,1:T(8,128)(2,1)} copy(bf16[2048,1024]{1,0:T(8,128)(2,1)} %get-tuple-element.9) | data formatting | bytes 8388608 | tf_op jit(solution)/shard_map/slice | solution.py:149
  105.6 0.0 copy-done.4
  105.6 3.7 fusion.17
  109.3 0.0 copy-done
  109.3 0.0 copy-start.8
  109.3 0.0 slice-start.1
  109.3 0.0 copy-start.7
  109.3 3.9 fusion.14
  113.2 0.0 copy-start.2
  113.2 0.0 copy-done.8
  113.3 0.0 slice-done
  113.3 0.0 slice-done.1
  113.3 5.0 %multiply_reduce_fusion = (f32[2,2048]{1,0:T(2,128)S(1)}, bf16[2,2048,128]{1,2,0:T(8,128)(2,1)}, f32[2,2048,128]{1,2,0:T(8,128)S(1)}) fusion(bf16[2,2048,128]{1,2,0:T(8,128)(2,1)S(1)} %fusion.17, bf16[2,2048,128]{1,2,0:T(8,128)(2,1)S(1)} %fusion.14, bf16[2,128,1024]{2,1,0:T(8,128)(2,1)S(1)} %copy-done.7, f32[2048,1024]{1,0:T(8,128)S(1)} %bitcast.16, ...), kind=kOutput, calls=%fused_computation.31 | convolution fusion | flops 1090514944 | bytes 14188544 | tf_op jit(solution)/shard_map/erd,efd->erf/dot_general | solution.py:15
  118.3 0.0 copy-done.2
  118.4 1.3 copy.78
  119.7 0.0 reduce-scatter.7.cloned.1.call-update
  119.7 0.2 reduce-scatter.5.cloned.1.call-start
  119.9 9.3 %fusion.30 = f32[2,2048,1024]{2,1,0:T(8,128)} fusion(bf16[2,2048,128]{1,2,0:T(8,128)(2,1)} %get-tuple-element.12, bf16[2,1024,128]{2,1,0:T(8,128)(2,1)S(1)} %copy-done), kind=kOutput, calls=%fused_computation.59 | convolution fusion | flops 1073741824 | bytes 18350080 | tf_op jit(solution)/shard_map/erf,edf->erd/dot_general | solution.py:28
  129.3 11.5 %add_reduce_fusion = f32[2048,1024]{1,0:T(8,128)} fusion(f32[2,2048,1024]{2,1,0:T(8,128)} %fusion.30, bf16[2,1024,128]{2,1,0:T(8,128)(2,1)S(1)} %copy-done.4, f32[2,2048,128]{1,2,0:T(8,128)S(1)} %get-tuple-element.13, bf16[2,2048,128]{1,2,0:T(8,128)(2,1)} %copy-done.2), kind=kOutput, calls=%fused_computation | convolution fusion | flops 1083703296 | bytes 28835840 | tf_op jit(solution)/shard_map/erf,edf->erd/dot_general | solution.py:31
  140.8 0.0 reduce-scatter.5.cloned.1.call-update
  140.8 0.0 copy-start.3
  140.9 0.0 slice-start.2
  140.9 5.9 %fusion.8 = f32[2,1024,128]{2,1,0:T(8,128)} fusion(bf16[2,2048,128]{1,2,0:T(8,128)(2,1)} %get-tuple-element.12, bf16[2048,1024]{0,1:T(8,128)(2,1)} %copy.60), kind=kOutput, calls=%fused_computation.11 | convolution fusion | flops 1073741824 | bytes 6291456 | tf_op jit(solution)/shard_map/erd,erf->edf/dot_general | solution.py:40
  146.8 0.0 copy-done.3
  146.8 3.4 fusion.6
  150.2 0.0 slice-done.2
  150.2 0.0 copy-start.5
  150.2 0.0 copy-start.6
  150.3 3.2 fusion
  153.5 101.5 %reduce-scatter.7.cloned.1.call-done = f32[64,16]{1,0:T(8,128)} async-done(((f32[2048,16]{1,0:T(8,128)}), f32[64,16]{1,0:T(8,128)}) %reduce-scatter.7.cloned.1.call-update) | async-done | bytes 4112
  255.0 0.8 copy.79
  255.8 5.2 %all-gather = f32[4,64,16]{1,2,0:T(8,128)S(1)} all-gather(f32[1,64,16]{1,2,0:T(8,128)S(1)} %bitcast.19), channel_id=1, replica_groups=mesh['ep'=8,'tp'=4] {'tp'}, dimensions={0}, use_global_device_ids=true | all-gather | bytes 20480 | tf_op jit(solution)/shard_map/all_gather | solution.py:162
  261.0 0.1 reshape.17
  261.1 0.0 copy-done.5
  261.1 0.0 copy-done.6
  261.2 0.6 div.7
  261.7 141.6 %reduce-scatter.5.cloned.1.call-done = f32[64,1024]{1,0:T(8,128)} async-done(((f32[2048,1024]{1,0:T(8,128)}), f32[64,1024]{1,0:T(8,128)}) %reduce-scatter.5.cloned.1.call-update) | async-done | bytes 262160 | tf_op jit(solution)/shard_map/reduce_scatter | solution.py:159
  403.3 1.0 convert_element_type.38
  404.3 6.5 %all_gather.10 = bf16[256,1024]{1,0:T(8,128)(2,1)S(1)} all-gather(bf16[64,1024]{1,0:T(8,128)(2,1)S(1)} %convert_element_type.38), channel_id=1, replica_groups=mesh['ep'=8,'tp'=4] {'tp'}, dimensions={0}, use_global_device_ids=true | all-gather | bytes 655360 | tf_op jit(solution)/shard_map/all_gather | solution.py:161
  410.8 0.8 copy.97
  (31 shorter events, 0.1 us)
Async XLA Ops:
  7.2 102.1 %copy-start = (bf16[2,1024,128]{2,1,0:T(8,128)(2,1)S(1)}, bf16[2,1024,128]{2,1,0:T(8,128)(2,1)}, u32[]{:S(2)}) copy-start(bf16[2,1024,128]{2,1,0:T(8,128)(2,1)} %param.11) | copy-start | bytes 1572868
  7.2 84.3 %all-gather.3.cloned.1.call-start = ((), (), s32[]{:S(2)}) async-start(), calls=%async_computation.2 | async-start | bytes 8650752 | tf_op jit(solution)/shard_map/all_gather | solution.py:138
  9.0 246.0 %reduce-scatter.7.cloned.1.call-start = ((), (), s32[]{:S(2)}) async-start(), calls=%async_computation.4 | async-start | bytes 1081344
  9.8 7.8 %collective-permute-start = (f32[256,16]{0,1:T(8,128)S(1)}, f32[256,16]{0,1:T(8,128)S(1)}, u32[]{:S(2)}, u32[]{:S(2)}) collective-permute-start(f32[256,16]{0,1:T(8,128)S(1)} %select_reduce_fusion.1), channel_id=1, source_target_pairs={{0,4},{4,8},{8,12},{12,16},{16,20},{20,24},{24,28},{28,0},{1,5},{5... | collective-permute-start | bytes 49160 | tf_op jit(solution)/shard_map/ppermute | solution.py:143
  17.6 6.4 %collective-permute-start.1 = (f32[256,16]{0,1:T(8,128)S(1)}, f32[256,16]{0,1:T(8,128)S(1)}, u32[]{:S(2)}, u32[]{:S(2)}) collective-permute-start(f32[256,16]{0,1:T(8,128)S(1)} %collective-permute-done), channel_id=1, source_target_pairs={{0,4},{4,8},{8,12},{12,16},{16,20},{20,24},{24,28},{28,0},{1,5},{5... | collective-permute-start | bytes 49160 | tf_op jit(solution)/shard_map/ppermute | solution.py:143
  24.0 6.5 %collective-permute-start.2 = (f32[256,16]{0,1:T(8,128)S(1)}, f32[256,16]{0,1:T(8,128)S(1)}, u32[]{:S(2)}, u32[]{:S(2)}) collective-permute-start(f32[256,16]{0,1:T(8,128)S(1)} %collective-permute-done.1), channel_id=1, source_target_pairs={{0,4},{4,8},{8,12},{12,16},{16,20},{20,24},{24,28},{28,0},{1,5},{5... | collective-permute-start | bytes 49160 | tf_op jit(solution)/shard_map/ppermute | solution.py:143
  30.5 6.5 %collective-permute-start.3 = (f32[256,16]{0,1:T(8,128)S(1)}, f32[256,16]{0,1:T(8,128)S(1)}, u32[]{:S(2)}, u32[]{:S(2)}) collective-permute-start(f32[256,16]{0,1:T(8,128)S(1)} %collective-permute-done.2), channel_id=1, source_target_pairs={{0,4},{4,8},{8,12},{12,16},{16,20},{20,24},{24,28},{28,0},{1,5},{5... | collective-permute-start | bytes 49160 | tf_op jit(solution)/shard_map/ppermute | solution.py:143
  37.0 6.6 %collective-permute-start.4 = (f32[256,16]{0,1:T(8,128)S(1)}, f32[256,16]{0,1:T(8,128)S(1)}, u32[]{:S(2)}, u32[]{:S(2)}) collective-permute-start(f32[256,16]{0,1:T(8,128)S(1)} %collective-permute-done.3), channel_id=1, source_target_pairs={{0,4},{4,8},{8,12},{12,16},{16,20},{20,24},{24,28},{28,0},{1,5},{5... | collective-permute-start | bytes 49160 | tf_op jit(solution)/shard_map/ppermute | solution.py:143
  43.6 6.9 %collective-permute-start.5 = (f32[256,16]{0,1:T(8,128)S(1)}, f32[256,16]{0,1:T(8,128)S(1)}, u32[]{:S(2)}, u32[]{:S(2)}) collective-permute-start(f32[256,16]{0,1:T(8,128)S(1)} %collective-permute-done.4), channel_id=1, source_target_pairs={{0,4},{4,8},{8,12},{12,16},{16,20},{20,24},{24,28},{28,0},{1,5},{5... | collective-permute-start | bytes 49160 | tf_op jit(solution)/shard_map/ppermute | solution.py:143
  50.6 6.6 %collective-permute-start.6 = (f32[256,16]{0,1:T(8,128)S(1)}, f32[256,16]{0,1:T(8,128)S(1)}, u32[]{:S(2)}, u32[]{:S(2)}) collective-permute-start(f32[256,16]{0,1:T(8,128)S(1)} %collective-permute-done.5), channel_id=1, source_target_pairs={{0,4},{4,8},{8,12},{12,16},{16,20},{20,24},{24,28},{28,0},{1,5},{5... | collective-permute-start | bytes 49160 | tf_op jit(solution)/shard_map/ppermute | solution.py:143
  99.0 6.6 %copy-start.4 = (bf16[2,1024,128]{2,1,0:T(8,128)(2,1)S(1)}, bf16[2,1024,128]{2,1,0:T(8,128)(2,1)}, u32[]{:S(2)}) copy-start(bf16[2,1024,128]{2,1,0:T(8,128)(2,1)} %param.12) | copy-start | bytes 1572868
  105.6 7.7 %slice-start = ((s8[8388608]{0:T(1024)(128)(4,1)}), s8[4194304]{0:T(1024)(128)(4,1)S(1)}, s32[]{:S(2)}) async-start(s8[8388608]{0:T(1024)(128)(4,1)} %bitcast.15), calls=%async_computation.5 | async-start | bytes 8388608
  109.3 4.0 copy-start.8
  109.3 4.0 slice-start.1
  109.3 4.0 copy-start.7
  113.2 5.1 %copy-start.2 = (bf16[2,2048,128]{1,2,0:T(8,128)(2,1)}, bf16[2,2048,128]{1,2,0:T(8,128)(2,1)S(1)}, u32[]{:S(2)}) copy-start(bf16[2,2048,128]{1,2,0:T(8,128)(2,1)S(1)} %fusion.14) | copy-start | bytes 3145732
  119.7 283.6 %reduce-scatter.5.cloned.1.call-start = ((), (), s32[]{:S(2)}) async-start(), calls=%async_computation.3 | async-start | bytes 8650752 | tf_op jit(solution)/shard_map/reduce_scatter | solution.py:159
  140.8 6.0 %copy-start.1 = (bf16[2048,1024]{0,1:T(8,128)(2,1)S(1)}, bf16[2048,1024]{0,1:T(8,128)(2,1)}, u32[]{:S(2)}) copy-start(bf16[2048,1024]{0,1:T(8,128)(2,1)} %copy.60) | copy-start | bytes 12582916
  140.8 6.0 %copy-start.3 = (bf16[2,2048,128]{1,2,0:T(8,128)(2,1)S(1)}, bf16[2,2048,128]{1,2,0:T(8,128)(2,1)}, u32[]{:S(2)}) copy-start(bf16[2,2048,128]{1,2,0:T(8,128)(2,1)} %copy-done.2) | copy-start | bytes 3145732
  140.9 9.4 %slice-start.2 = ((s8[8388608]{0:T(1024)(128)(4,1)}), s8[4194304]{0:T(1024)(128)(4,1)S(1)}, s32[]{:S(2)}) async-start(s8[8388608]{0:T(1024)(128)(4,1)} %bitcast.17), calls=%async_computation.7 | async-start | bytes 8388608
  146.8 3.4 slice-start.3
  146.8 3.4 copy-start.9
  150.2 110.9 %copy-start.5 = (s32[256,2]{0,1:T(2,128)S(1)}, s32[256,2]{0,1:T(2,128)}, u32[]{:S(2)}) copy-start(s32[256,2]{0,1:T(2,128)} %param.9) | copy-start | bytes 6148
  150.2 110.9 %copy-start.6 = (f32[256,2]{0,1:T(2,128)S(1)}, f32[256,2]{0,1:T(2,128)}, u32[]{:S(2)}) copy-start(f32[256,2]{0,1:T(2,128)} %param.10) | copy-start | bytes 6148
Sparse Core Ops, SparseCore 0:
  11.4 80.0 all-gather.2
  119.8 135.1 reduce-scatter.6
  257.3 145.9 reduce-scatter.4
